TPU v7x, 256 devices: a whole 4x4x8 slice. The times are simulated.
256 devices in a mesh: dp: 4 (over y), kv: 32 (over z, x), tp: 2 (over core).
Axes of the slice: x: 4, y: 4, z: 8, core: 2. Of those that a mesh axis runs over, the one named last changes fastest.
Arguments:
- tokens: bfloat16 [1024, 4096], P('dp', ('kv', 'tp')), may hold values from -11.5 to 11.5, as said below
- gain_mix: float32 [4096], replicated, may hold values from 0.1 to 1.9
- gain_mlp: float32 [4096], replicated, may hold values from 0.1 to 1.9
- decay_rate: float32 [16], replicated, may hold values from 0.01 to 1
- w_query: bfloat16 [4096, 1024], P('kv', 'tp'), may hold values from -0.09375 to 0.09375
- w_key: bfloat16 [4096, 1024], P('kv', 'tp'), may hold values from -0.09375 to 0.09375
- w_value: bfloat16 [4096, 2048], P('kv', 'tp'), may hold values from -0.09375 to 0.09375
- w_gate: bfloat16 [4096, 2048], P('kv', 'tp'), may hold values from -0.09375 to 0.09375
- w_mix: bfloat16 [2048, 4096], P('tp', 'kv'), may hold values from -0.125 to 0.125
- w_up: bfloat16 [4096, 16384], P(None, ('kv', 'tp')), may hold values from -0.09375 to 0.09375
- w_down: bfloat16 [16384, 4096], P(('kv', 'tp')), may hold values from -0.125 to 0.125
- state: float32 [1024, 16, 64, 128], P(('dp', 'kv'), 'tp'), may hold values from -2 to 2
Outputs:
- result: bfloat16 [1024, 4096], P('dp', ('kv', 'tp'))
- new_state: float32 [1024, 16, 64, 128], P(('dp', 'kv'), 'tp')
Inputs may be any that keep to these rules, and one draw needn't show every extreme that they name: `tokens`: feature scales differ across the features.
All inputs are finite; a program needn't handle non-finite values.
Results may differ from a plain program's by a relative error of at most 0.02.
Values may be sent and summed in bfloat16 or wider, within the bound.
No kernel may reach another device: no remote copies, remote signals or barrier semaphores. Data moves between devices by JAX's collectives and lax.ppermute only.
A program may use at most 64 MiB of HBM per device.

v0:
```python
import jax
import jax.numpy as jnp
from jax import lax
from jax.experimental import pallas as pl
from jax.experimental.pallas import tpu as pltpu
from jax.sharding import Mesh
from jax.sharding import PartitionSpec as P

KV = ("kv_0", "kv_1")
KV_TP = ("kv_0", "kv_1", "tp")
DP_KV = ("dp", "kv_0", "kv_1")

EPS = 1e-06
F32 = jnp.float32
BF16 = jnp.bfloat16
LANES = 128


def dot(a, b):
    return jnp.dot(a, b, preferred_element_type=F32)


def kernel_call(body, outs, *args, scratch=(), hbm=(), flops=0, bytes_accessed=0):
    vmem = pl.BlockSpec(memory_space=pltpu.VMEM)
    in_hbm = pl.BlockSpec(memory_space=pltpu.HBM)
    return pl.pallas_call(
        body,
        out_shape=[jax.ShapeDtypeStruct(*o) for o in outs],
        in_specs=[in_hbm if i in hbm else vmem for i in range(len(args))],
        out_specs=[vmem] * len(outs),
        scratch_shapes=list(scratch),
        compiler_params=pltpu.CompilerParams(vmem_limit_bytes=10 * 2**20),
        cost_estimate=pl.CostEstimate(
            flops=flops, bytes_accessed=bytes_accessed, transcendentals=0
        ),
    )(*args)


def swap_tp(x):
    return lax.ppermute(x, "tp", [(0, 1), (1, 0)])


def ring_sizes():
    return lax.axis_size("kv_0"), lax.axis_size("kv_1")


def own_class():
    return 2 * (lax.axis_index("kv_0") % 2) + lax.axis_index("kv_1") % 2


def members(z_size, x_size):
    return [(zr, xr) for zr in range(z_size // 2) for xr in range(x_size // 2)]


def member_kv(member, which, x_size):
    return (2 * member[0] + which // 2) * x_size + 2 * member[1] + which % 2


def class_groups():
    z_size, x_size = ring_sizes()
    return [
        [member_kv(m, c, x_size) * 2 + tp for m in members(z_size, x_size)]
        for tp in range(2)
        for c in range(4)
    ]


def to_neighbour(x, place, split=True):
    z_size, x_size = ring_sizes()

    def across(position, tp, size):
        return (position + (1 if position % 2 == tp * split else -1)) % size

    pairs = []
    for z in range(z_size):
        for x_ in range(x_size):
            for tp in range(2):
                to_z = across(z, tp, z_size) if place & 2 else z
                to_x = across(x_, tp, x_size) if place & 1 else x_
                pairs.append(((z * x_size + x_) * 2 + tp, (to_z * x_size + to_x) * 2 + tp))
    return lax.ppermute(x, KV_TP, pairs)


def in_class(x):
    return lax.all_to_all(x, KV_TP, 0, 0, axis_index_groups=class_groups(), tiled=True)


PLACES = (3, 1, 2)


def sum_in_square(parts):
    arrived = {}
    for place in PLACES:
        arrived[place] = to_neighbour(parts[place], place)
    total = parts[0].astype(F32)
    for place in PLACES:
        total = total + arrived[place].astype(F32)
    return total.astype(BF16)


def from_square(own):
    arrived = {place: to_neighbour(own, place) for place in PLACES}
    return [own, *(arrived[place] for place in (1, 2, 3))]


def fetch_kernel(*refs):
    count = len(refs) // 2
    sem = refs[-1]
    copies = [
        pltpu.make_async_copy(refs[i], refs[count + i], sem.at[i]) for i in range(count)
    ]
    for copy in copies:
        copy.start()
    for copy in copies:
        copy.wait()


def inputs_kernel(other, own, gain, w_query, w_key, w_value, w_gate, *rest, sizes):
    outs, tokens_out, by_class = rest[:4], rest[4], rest[5]
    tp = lax.axis_index("tp")
    kv = lax.axis_index(KV)
    first, second = own[...].astype(F32), other[...].astype(F32)
    both = jnp.where(
        tp == 0,
        jnp.concatenate([first, second], axis=0),
        jnp.concatenate([second, first], axis=0),
    ).T
    seqs = both.shape[0] // (sizes[0] * sizes[1])
    for c in range(4):
        kvs = [member_kv(m, c, sizes[1]) for m in members(*sizes)]
        by_class[c] = jnp.concatenate([both[i * seqs : (i + 1) * seqs] for i in kvs], axis=0)
    for place in range(4):
        tokens_out[place] = by_class[own_class() ^ place].astype(BF16)
    both = jnp.concatenate([by_class[own_class() ^ place] for place in range(4)], axis=0)
    squares = jnp.sum(both * both, axis=1, keepdims=True)
    high = squares.astype(BF16).astype(F32)
    low = squares - high
    lane = lax.broadcasted_iota(jnp.int32, (squares.shape[0], LANES), 1)
    scaled = (both * gain[pl.ds(kv, 1), :]).astype(BF16)
    start = 0
    for weight in (w_query, w_key, w_value, w_gate):
        width = weight.shape[1]
        product = dot(scaled, weight[...]).astype(BF16)
        for place, out in enumerate(outs):
            count = out.shape[0]
            out[:, start : start + width] = product[place * count : (place + 1) * count]
        start += width
    totals = jnp.where(lane == 0, high, jnp.where(lane == 1, low, 0.0)).astype(BF16)
    for place, out in enumerate(outs):
        count = out.shape[0]
        out[:, start : start + LANES] = totals[place * count : (place + 1) * count]


def decay_kernel(state, rates, out):
    heads = rates.shape[0]
    decay = jnp.exp(-rates[...])
    for i in range(out.shape[0]):
        h = i % heads
        out[i] = decay[h : h + 1, :] * state[i]


def retention_kernel(
    parts, decayed, heads_out, key_out, value_out, read_ref, *, model_width, sizes
):
    seqs, heads, key_width, value_width = sizes
    total = parts[0].astype(F32)
    for j in range(1, parts.shape[0]):
        total = total + parts[j].astype(F32)
    q_end = heads * key_width
    k_end = 2 * q_end
    v_end = k_end + heads * value_width
    g_end = v_end + heads * value_width
    row_total = total[:, g_end : g_end + 1] + total[:, g_end + 1 : g_end + 2]
    scale = lax.rsqrt(row_total / model_width + EPS)

    def rounded(x):
        return (x * scale).astype(BF16).astype(F32)

    query = rounded(total[:, :q_end])
    key = rounded(total[:, q_end:k_end]) * key_width ** (-0.5)
    value = rounded(total[:, k_end:v_end])
    gate = rounded(total[:, v_end:g_end])
    query_t = query.T
    key_out[...] = key.T
    value_out[...] = value
    for b in range(seqs):
        for h in range(heads):
            rows = slice(h * key_width, (h + 1) * key_width)
            cols = slice(h * value_width, (h + 1) * value_width)
            read_ref[b : b + 1, cols] = jnp.sum(
                query_t[rows, b : b + 1] * decayed[b * heads + h], axis=0, keepdims=True
            )
    for h in range(heads):
        rows = slice(h * key_width, (h + 1) * key_width)
        cols = slice(h * value_width, (h + 1) * value_width)
        match = jnp.sum(query[:, rows] * key[:, rows], axis=1, keepdims=True)
        read = read_ref[:, cols] + match * value[:, cols]
        read = read * lax.rsqrt(jnp.mean(read * read, axis=1, keepdims=True) + EPS)
        g = gate[:, cols]
        done = (g / (1.0 + jnp.exp(-g)) * read).astype(BF16)
        for j in range(heads_out.shape[0]):
            heads_out[j, :, cols] = done


def state_kernel(decayed, key_t, value, new_state):
    seqs, width = value.shape
    key_width, value_width = decayed.shape[1:]
    heads = width // value_width
    for b in range(seqs):
        for h in range(heads):
            rows = slice(h * key_width, (h + 1) * key_width)
            cols = slice(h * value_width, (h + 1) * value_width)
            new_state[b * heads + h] = (
                decayed[b * heads + h] + key_t[rows, b : b + 1] * value[b : b + 1, cols]
            )


def pack_kernel(w_mix, tokens, *packs):
    depth = w_mix.shape[0]
    for place, pack in enumerate(packs, 1):
        pack[:depth, :] = w_mix[...]
        pack[depth:, :] = tokens[place]


def copy_kernel(x, out):
    out[...] = x[0]


def mix_kernel(heads, w_mix, *rest):
    packs, (keep, send, product) = rest[:3], rest[3:]
    tp = lax.axis_index("tp")
    depth = w_mix.shape[0]
    half = keep.shape[1]
    weights = [w_mix[...], *(pack[:depth, :] for pack in packs)]
    width = w_mix.shape[1]
    for place in (0, 2):
        pair = dot(heads[...], jnp.concatenate(weights[place : place + 2], axis=1))
        product[own_class() ^ place] = pair[:, :width]
        product[own_class() ^ (place + 1)] = pair[:, width:]
    for c in range(4):
        keep[c] = product[c, pl.ds(pl.multiple_of(tp * half, half), half), :].astype(BF16)
        send[c] = product[c, pl.ds(pl.multiple_of((1 - tp) * half, half), half), :].astype(BF16)


def resid_kernel(tokens, *rest):
    packs, (keep, received, out) = rest[:3], rest[3:]
    half = keep.shape[1]
    depth = packs[0].shape[0] - 2 * half
    start = pl.multiple_of(lax.axis_index("tp") * half, half)
    for place in range(4):
        c = own_class() ^ place
        if place:
            own = packs[place - 1][pl.ds(depth + start, half), :]
        else:
            own = tokens[pl.ds(start, half), :]
        mixed = keep[c].astype(F32) + received[c].astype(F32)
        resid = (own.astype(F32) + mixed).astype(BF16)
        for j in range(out.shape[0]):
            out[j, c] = resid


def up_kernel(*refs, sizes, model_width):
    places = (len(refs) - 3) // 2
    mine, other, (gain, w_up, hidden) = refs[:places], refs[places : 2 * places], refs[-3:]
    _, classes, half, width = mine[0].shape
    pieces = [*mine, *other]
    total = jnp.zeros((len(pieces) * half, w_up.shape[1]), F32)
    square = jnp.zeros((len(pieces) * half, width), F32)
    for i, m in enumerate(members(*sizes)):
        for c in range(0, classes, 2):
            blocks, weights = [], []
            for which in (c, c + 1):
                kv = member_kv(m, which, sizes[1])
                block = jnp.concatenate([x[i, which] for x in pieces], axis=0).astype(F32)
                square = square + block * block
                blocks.append((block * gain[kv : kv + 1, :]).astype(BF16))
                weights.append(w_up[kv * width : (kv + 1) * width, :])
            total = total + dot(
                jnp.concatenate(blocks, axis=1), jnp.concatenate(weights, axis=0)
            )
    scale = lax.rsqrt(jnp.sum(square, axis=1, keepdims=True) / model_width + EPS)
    total = jnp.maximum(total * scale, 0.0)
    hidden[...] = (total * total).astype(BF16)


def hidden_in_order(first, second, out, first_places, second_places):
    rows = out.shape[0] // 8
    for ref, places in ((first, first_places), (second, second_places)):
        for owner in range(2):
            for i, place in enumerate(places):
                start = (owner * len(places) + i) * rows
                to = owner * 4 * rows + (own_class() ^ place) * rows
                out[pl.ds(pl.multiple_of(to, rows), rows), :] = ref[start : start + rows, :]


def own_lanes(half, width):
    lane = lax.broadcasted_iota(jnp.int32, (half, width), 1)
    return jnp.where(lane < width // 2, 0, 1) == lax.axis_index("tp")


def down_kernel(hidden, w_down, keep, send, *, place, sizes):
    count, half, width = keep.shape
    own = own_lanes(half, width)
    for j in range(0, count, 2):
        weights = []
        for i in (j, j + 1):
            kv = member_kv(members(*sizes)[i], own_class() ^ place, sizes[1])
            weights.append(w_down[:, pl.ds(pl.multiple_of(kv * width, width), width)])
        pair = dot(hidden[...], jnp.concatenate(weights, axis=1))
        for i in (j, j + 1):
            cols = slice((i - j) * width, (i - j + 1) * width)
            from_mine, from_other = pair[:half, cols], pair[half:, cols]
            keep[i] = jnp.where(own, from_mine, pltpu.roll(from_other, width // 2, 1))
            send[i] = jnp.where(own, pltpu.roll(from_mine, width // 2, 1), from_other).astype(BF16)


def own_resid_kernel(*refs, sizes):
    mine, other, resid = refs[:4], refs[4:8], refs[8]
    kv = lax.axis_index(KV)
    spot = (kv // sizes[1] // 2) * (sizes[1] // 2) + kv % sizes[1] // 2
    rows, width = mine[0].shape[2:]
    for place in range(4):
        to = (own_class() ^ place) * rows
        resid[pl.ds(pl.multiple_of(to, rows), rows), :] = jnp.where(
            own_lanes(rows, width),
            mine[place][spot, own_class()].astype(F32),
            pltpu.roll(other[place][spot, own_class()].astype(F32), width // 2, 1),
        )


def result_kernel(parts, resid, out, *, sizes):
    half, width = resid.shape
    total = parts[0].astype(F32)
    for j in range(1, parts.shape[0]):
        total = total + parts[j].astype(F32)
    total = resid[...] + total
    halves = (total, pltpu.roll(total, width // 2, 1))
    count = len(members(*sizes))
    seqs = half // (2 * count)
    blocks = {}
    for i, m in enumerate(members(*sizes)):
        for c in range(4):
            start = (c * (count // 2) + i % (count // 2)) * seqs
            blocks[member_kv(m, c, sizes[1])] = halves[i // (count // 2)][start : start + seqs]
    rows = jnp.concatenate([blocks[kv] for kv in range(len(blocks))], axis=0)
    out[...] = rows.T[: width // 2].astype(BF16)


def layer(
    tokens,
    gain_mix,
    gain_mlp,
    decay_rate,
    w_query,
    w_key,
    w_value,
    w_gate,
    w_mix,
    w_up,
    w_down,
    state,
):
    seqs, heads, key_width, value_width = state.shape
    rows, own_cols = tokens.shape
    half = rows // 2
    cols = 2 * own_cols
    peers = lax.axis_size(KV)
    model_width = cols * peers
    sizes = ring_sizes()
    count = peers // 4
    qkvg = sum(w.shape[1] for w in (w_query, w_key, w_value, w_gate))
    payload_width = qkvg + LANES
    tokens_t = tokens.T

    def inputs_body(*refs):
        inputs_kernel(*refs, sizes=sizes)

    sources = [
        pltpu.with_memory_space_constraint(x, pltpu.HBM)
        for x in (tokens_t, gain_mix.reshape(peers, cols), w_query, w_key, w_value, w_gate)
    ]
    depth = w_mix.shape[0]
    fetched = kernel_call(
        fetch_kernel,
        [(x.shape, x.dtype) for x in sources],
        *sources,
        hbm=range(len(sources)),
        scratch=[pltpu.SemaphoreType.DMA((len(sources),))],
        flops=10**7,
        bytes_accessed=2**21,
    )
    *payload, own_tokens = kernel_call(
        inputs_body,
        [((rows // 4, payload_width), BF16)] * 4 + [((4, rows // 4, cols), BF16)],
        swap_tp(tokens_t),
        *fetched,
        scratch=[pltpu.VMEM((4, rows // 4, cols), F32)],
    )
    rates = lax.dynamic_slice_in_dim(decay_rate, lax.axis_index("tp") * heads, heads)
    (decayed,) = kernel_call(
        decay_kernel,
        [((seqs * heads, key_width, value_width), F32)],
        state.reshape(seqs * heads, key_width, value_width),
        jnp.broadcast_to(rates[:, None], (heads, value_width)),
        flops=3 * 10**7,
        bytes_accessed=2**23,
    )
    total = sum_in_square([piece.reshape(count, seqs, payload_width) for piece in payload])
    total, decayed = lax.optimization_barrier((total, decayed))
    packs = kernel_call(
        pack_kernel,
        [((depth + rows // 4, cols), BF16)] * 3,
        w_mix,
        own_tokens,
        flops=10**6,
        bytes_accessed=2**21,
    )
    (own_piece,) = kernel_call(copy_kernel, [((rows // 4, cols), BF16)], own_tokens)
    near_packs = {}
    for place in PLACES:
        near_packs[place] = to_neighbour(packs[place - 1], place, split=False)
    packs = [near_packs[place] for place in (1, 2, 3)]
    parts = in_class(total)

    def retention_body(*refs):
        retention_kernel(
            *refs, model_width=model_width, sizes=(seqs, heads, key_width, value_width)
        )

    heads_out, key_t, value = kernel_call(
        retention_body,
        [
            ((count, seqs, heads * value_width), BF16),
            ((heads * key_width, seqs), F32),
            ((seqs, heads * value_width), F32),
        ],
        parts,
        decayed,
        scratch=[pltpu.VMEM((seqs, heads * value_width), F32)],
    )
    far_heads = in_class(heads_out)
    key_t, far_heads = lax.optimization_barrier((key_t, far_heads))
    (new_state,) = kernel_call(
        state_kernel,
        [((seqs * heads, key_width, value_width), F32)],
        decayed,
        key_t,
        value,
        flops=3 * 10**7,
        bytes_accessed=2**23,
    )

    quarter = (4, rows // 8, cols)
    keep, send = kernel_call(
        mix_kernel,
        [(quarter, BF16)] * 2,
        far_heads.reshape(rows // 4, heads * value_width),
        w_mix,
        *packs,
        scratch=[pltpu.VMEM((4, rows // 4, cols), F32)],
    )
    (resid,) = kernel_call(
        resid_kernel, [((count, *quarter), BF16)], own_piece, *packs, keep, swap_tp(send)
    )
    mine = from_square(in_class(resid))
    other = [swap_tp(x) for x in mine]
    gains = gain_mlp.reshape(peers, cols)

    def up_body(*refs):
        up_kernel(*refs, sizes=sizes, model_width=model_width)

    early, late = (0, 3), (1, 2)
    hiddens = []
    for places in (early, late):
        (hidden,) = kernel_call(
            up_body,
            [((2 * len(places) * rows // 8, w_up.shape[1]), BF16)],
            *(mine[place] for place in places),
            *(other[place] for place in places),
            gains,
            w_up,
            flops=10**7,
            bytes_accessed=2**21,
        )
        hiddens.append(hidden)

    def own_resid_body(*refs):
        own_resid_kernel(*refs, sizes=sizes)

    (own_resid,) = kernel_call(
        own_resid_body, [((half, cols), F32)], *mine, *other, flops=10**5
    )
    piece = (count, half, cols)
    chip_sum = {}
    hidden = None
    for place in (*PLACES, 0):

        def down_body(*refs, place=place):
            down_kernel(*refs, place=place, sizes=sizes)

        def first_down_body(*refs, place=place):
            hidden_ref = refs[-1]
            hidden_in_order(*refs[:2], hidden_ref, early, late)
            down_kernel(hidden_ref, *refs[2:-1], place=place, sizes=sizes)

        outs = [(piece, F32), (piece, BF16)]
        if hidden is None:
            keep, send, hidden = kernel_call(
                first_down_body, [*outs, ((rows, w_up.shape[1]), BF16)], *hiddens, w_down
            )
        else:
            keep, send = kernel_call(
                down_body, outs, hidden, w_down, flops=10**7, bytes_accessed=2**21
            )
        chip_sum[place] = (keep + swap_tp(send).astype(F32)).astype(BF16)
    total, own_resid, new_state = lax.optimization_barrier(
        (sum_in_square(chip_sum), own_resid, new_state)
    )
    parts = in_class(total)

    def result_body(*refs):
        result_kernel(*refs, sizes=sizes)

    (result_t,) = kernel_call(result_body, [((own_cols, rows), BF16)], parts, own_resid)
    return (result_t.T, new_state.reshape(state.shape))


def solution(mesh):
    torus = Mesh(
        mesh.devices.reshape(mesh.shape["dp"], 8, 4, mesh.shape["tp"]), ("dp", "kv_0", "kv_1", "tp")
    )
    return jax.shard_map(
        layer,
        mesh=torus,
        in_specs=(
            P("dp", KV_TP),
            P(),
            P(),
            P(),
            P(KV, "tp"),
            P(KV, "tp"),
            P(KV, "tp"),
            P(KV, "tp"),
            P("tp", KV),
            P(None, KV_TP),
            P(KV_TP, None),
            P(DP_KV, "tp", None, None),
        ),
        out_specs=(P("dp", KV_TP), P(DP_KV, "tp", None, None)),
        check_vma=False,
    )
```

profile of v0, /device:TPU:80, one launch (start us, length us, event | category | flops | bytes accessed | tf_op | source)
XLA Modules:
  0.0 122.9 jit_solution(13477061622594963002)
XLA Ops:
  0.7 1.2 %shard_map.131 = (bf16[64,256]{1,0:T(8,128)(2,1)S(1)}, f32[32,128]{1,0:T(8,128)S(1)}, bf16[128,512]{1,0:T(8,128)(2,1)S(1)}, bf16[128,512]{1,0:T(8,128)(2,1)S(1)}...) custom-call(bf16[64,256]{1,0:T(8,128)(2,1)} %bitcast.20, f32[32,128]{1,0:T(8,128)} %bitcast.22, ...), custom_call_target="tpu_custom_call" | custom-call | flops 10000000 | bytes 2097152 | tf_op jit(solution)/shard_map/pallas_call | solution.py:26
  2.1 1.5 %shard_map.132 = (bf16[64,3200]{1,0:T(8,128)(2,1)S(1)}, bf16[64,3200]{1,0:T(8,128)(2,1)}, bf16[64,3200]{1,0:T(8,128)(2,1)S(1)}, bf16[64,3200]{1,0:T(8,128)(2,1)}, bf16[4,64,128]{2,1,0:T(8,128)(2,1)S(1)}) custom-call(bf16[64,256]{1,0:T(8,128)(2,1)S(1)} %collective-permute-done.refs_0_, bf16[64,256]{1,0:T(8,128)(2,1)S(1)} %get-tuple-element.37.refs_1_, ...), custom_call_target="tpu_custom_call" | custom-call | tf_op jit(solution)/shard_map/pallas_call | solution.py:26
  3.7 2.8 %collective-permute-start.4 = (bf16[8,8,3200]{2,1,0:T(8,128)(2,1)}, bf16[8,8,3200]{2,1,0:T(8,128)(2,1)}, u32[]{:S(2)}, u32[]{:S(2)}) collective-permute-start(bf16[8,8,3200]{2,1,0:T(8,128)(2,1)} %bitcast.3), channel_id=1, source_target_pairs={{0,10},{1,63},{2,8},{3,61},{4,14},{5,59},{6,12},{7,57},{8,2},{9,23... | collective-permute-start | bytes 1228808 | tf_op jit(solution)/shard_map/ppermute | solution.py:81
  7.1 0.7 dynamic_slice.3
  7.9 1.6 %copy-done.2 = f32[8,8,64,128]{3,2,1,0:T(8,128)S(1)} copy-done((f32[8,8,64,128]{3,2,1,0:T(8,128)S(1)}, f32[8,8,64,128]{3,2,1,0:T(8,128)}, u32[]{:S(2)}) %copy-start.2) | copy-done | bytes 2097176
  9.7 3.2 %collective-permute-done.4 = bf16[8,8,3200]{2,1,0:T(8,128)(2,1)} collective-permute-done((bf16[8,8,3200]{2,1,0:T(8,128)(2,1)}, bf16[8,8,3200]{2,1,0:T(8,128)(2,1)}, u32[]{:S(2)}, u32[]{:S(2)}) %collective-permute-start.4) | collective-permute-done | bytes 409632 | tf_op jit(solution)/shard_map/ppermute | solution.py:81
  12.9 4.3 %collective-permute-done.5 = bf16[8,8,3200]{2,1,0:T(8,128)(2,1)} collective-permute-done((bf16[8,8,3200]{2,1,0:T(8,128)(2,1)}, bf16[8,8,3200]{2,1,0:T(8,128)(2,1)}, u32[]{:S(2)}, u32[]{:S(2)}) %collective-permute-start.5) | collective-permute-done | bytes 409632 | tf_op jit(solution)/shard_map/ppermute | solution.py:81
  17.3 2.2 %fusion.2 = bf16[8,8,3200]{2,1,0:T(8,128)(2,1)} fusion(bf16[8,8,3200]{2,1,0:T(8,128)(2,1)} %collective-permute-done.6, bf16[8,8,3200]{2,1,0:T(8,128)(2,1)} %collective-permute-done.5, bf16[8,8,3200]{2,1,0:T(8,128)(2,1)} %collective-permute-done.4, bf16[64,3200]{1,0:T(8,128)(2,1)S(1)} %get-tuple-element.47), kind=kLoop, calls=%fused_computation.3 | loop fusion | flops 1638400 | bytes 2048000 | tf_op jit(solution)/shard_map/convert_element_type | solution.py:98
  19.5 10.5 %all-to-all-start = ((bf16[8,8,3200]{2,1,0:T(8,128)(2,1)}), bf16[8,8,3200]{2,1,0:T(8,128)(2,1)S(1)}, u32[]{:S(2)}, u32[]{:S(2)}) async-start(bf16[8,8,3200]{2,1,0:T(8,128)(2,1)} %fusion.2), calls=%async_computation | async-start | bytes 819200 | tf_op jit(solution)/shard_map/all_to_all | solution.py:85
  30.0 1.0 shard_map.134
  31.0 0.6 collective-permute-start.1
  31.6 1.0 collective-permute-start.2
  32.6 1.9 %collective-permute-start.3 = (bf16[1088,128]{1,0:T(8,128)(2,1)}, bf16[1088,128]{1,0:T(8,128)(2,1)S(1)}, u32[]{:S(2)}, u32[]{:S(2)}) collective-permute-start(bf16[1088,128]{1,0:T(8,128)(2,1)} %get-tuple-element.46), channel_id=1, source_target_pairs={{0,10},{1,11},{2,8},{3,9},{4,14},{5,15},{6,12},{7,13},{8,2},{9,3},... | collective-permute-start | bytes 835592 | tf_op jit(solution)/shard_map/ppermute | solution.py:81
  34.5 8.6 %all-to-all-done.refs_0_ = bf16[8,8,3200]{2,1,0:T(8,128)(2,1)S(1)} async-done(((bf16[8,8,3200]{2,1,0:T(8,128)(2,1)}), bf16[8,8,3200]{2,1,0:T(8,128)(2,1)S(1)}, u32[]{:S(2)}, u32[]{:S(2)}) %all-to-all-start) | async-done | bytes 409632 | tf_op jit(solution)/shard_map/all_to_all | solution.py:85
  43.1 0.8 shard_map.136
  44.0 15.2 %all_to_all.20 = bf16[8,8,1024]{2,1,0:T(8,128)(2,1)S(1)} all-to-all(bf16[8,8,1024]{2,1,0:T(8,128)(2,1)S(1)} %get-tuple-element.54), channel_id=1, replica_groups={{0,4,16,20,32,36,48,52},{2,6,18,22,34,38,50,54},{8,12,24,28,40,44,56,60..., dimensions={0} | all-to-all | bytes 262144 | tf_op jit(solution)/shard_map/all_to_all | solution.py:85
  59.6 1.2 collective-permute-done.7.rest_4_
  60.8 16.8 %all_to_all.21.refs_0_ = bf16[8,4,32,128]{3,2,1,0:T(8,128)(2,1)S(1)} all-to-all(bf16[8,4,32,128]{3,2,1,0:T(8,128)(2,1)S(1)} %shard_map.138), channel_id=1, replica_groups={{0,4,16,20,32,36,48,52},{2,6,18,22,34,38,50,54},{8,12,24,28,40,44,56,60..., dimensions={0} | all-to-all | bytes 524288 | tf_op jit(solution)/shard_map/all_to_all | solution.py:85
  77.6 0.9 collective-permute-start.11
  78.5 2.5 %collective-permute-start.8 = (bf16[8,4,32,128]{3,2,1,0:T(8,128)(2,1)S(1)}, bf16[8,4,32,128]{3,2,1,0:T(8,128)(2,1)S(1)}, u32[]{:S(2)}, u32[]{:S(2)}) collective-permute-start(bf16[8,4,32,128]{3,2,1,0:T(8,128)(2,1)S(1)} %all_to_all.21.refs_0_), channel_id=1, source_target_pairs={{0,10},{1,63},{2,8},{3,61},{4,14},{5,59},{6,12},{7,57},{8,2},{9,23... | collective-permute-start | bytes 786440 | tf_op jit(solution)/shard_map/ppermute | solution.py:81
  81.1 2.9 %collective-permute-done.11.refs_0_.refs_1_ = bf16[8,4,32,128]{3,2,1,0:T(8,128)(2,1)S(1)} collective-permute-done((bf16[8,4,32,128]{3,2,1,0:T(8,128)(2,1)S(1)}, bf16[8,4,32,128]{3,2,1,0:T(8,128)(2,1)S(1)}, u32[]{:S(2)}, u32[]{:S(2)}) %collective-permute-start.11) | collective-permute-done | bytes 262176 | tf_op jit(solution)/shard_map/ppermute | solution.py:81
  84.0 0.9 collective-permute-done.12.refs_1_.refs_2_
  85.4 2.8 %collective-permute-done.8.refs_1_.refs_3_ = bf16[8,4,32,128]{3,2,1,0:T(8,128)(2,1)S(1)} collective-permute-done((bf16[8,4,32,128]{3,2,1,0:T(8,128)(2,1)S(1)}, bf16[8,4,32,128]{3,2,1,0:T(8,128)(2,1)S(1)}, u32[]{:S(2)}, u32[]{:S(2)}) %collective-permute-start.8) | collective-permute-done | bytes 262176 | tf_op jit(solution)/shard_map/ppermute | solution.py:81
  88.8 1.0 collective-permute-done.10.refs_3_.refs_7_
  90.9 0.6 collective-permute-start.16
  94.4 1.3 %collective-permute-start.19 = (bf16[8,128,128]{2,1,0:T(8,128)(2,1)S(1)}, bf16[8,128,128]{2,1,0:T(8,128)(2,1)S(1)}, u32[]{:S(2)}, u32[]{:S(2)}) collective-permute-start(bf16[8,128,128]{2,1,0:T(8,128)(2,1)S(1)} %add_convert_fusion.2), channel_id=1, source_target_pairs={{0,2},{1,7},{2,0},{3,5},{4,6},{5,3},{6,4},{7,1},{8,10},{9,15},{10,... | collective-permute-start | bytes 786440 | tf_op jit(solution)/shard_map/ppermute | solution.py:81
  95.8 2.0 %collective-permute-start.21 = (bf16[8,128,128]{2,1,0:T(8,128)(2,1)S(1)}, bf16[8,128,128]{2,1,0:T(8,128)(2,1)S(1)}, u32[]{:S(2)}, u32[]{:S(2)}) collective-permute-start(bf16[8,128,128]{2,1,0:T(8,128)(2,1)S(1)} %add_convert_fusion.1), channel_id=1, source_target_pairs={{0,8},{1,57},{2,10},{3,59},{4,12},{5,61},{6,14},{7,63},{8,0},{9,17... | collective-permute-start | bytes 786440 | tf_op jit(solution)/shard_map/ppermute | solution.py:81
  97.8 1.9 %shard_map.146 = f32[64,64,128]{2,1,0:T(8,128)} custom-call(f32[64,64,128]{2,1,0:T(8,128)S(1)} %shard_map.135.refs_1_.decayed, f32[512,8]{1,0:T(8,128)S(1)} %get-tuple-element.67.key_t, f32[8,1024]{1,0:T(8,128)S(1)} %get-tuple-element.68.value), custom_call_target="tpu_custom_call" | custom-call | flops 30000000 | bytes 8388608 | tf_op jit(solution)/shard_map/pallas_call | solution.py:26
  99.8 1.5 %collective-permute-done.17 = bf16[8,128,128]{2,1,0:T(8,128)(2,1)S(1)} collective-permute-done((bf16[8,128,128]{2,1,0:T(8,128)(2,1)S(1)}, bf16[8,128,128]{2,1,0:T(8,128)(2,1)S(1)}, u32[]{:S(2)}, u32[]{:S(2)}) %collective-permute-start.17) | collective-permute-done | bytes 262176 | tf_op jit(solution)/shard_map/ppermute | solution.py:81
  101.4 2.3 %collective-permute-done.19 = bf16[8,128,128]{2,1,0:T(8,128)(2,1)S(1)} collective-permute-done((bf16[8,128,128]{2,1,0:T(8,128)(2,1)S(1)}, bf16[8,128,128]{2,1,0:T(8,128)(2,1)S(1)}, u32[]{:S(2)}, u32[]{:S(2)}) %collective-permute-start.19) | collective-permute-done | bytes 262176 | tf_op jit(solution)/shard_map/ppermute | solution.py:81
  103.9 18.2 %all_to_all.22.refs_0_ = bf16[8,128,128]{2,1,0:T(8,128)(2,1)S(1)} all-to-all(bf16[8,128,128]{2,1,0:T(8,128)(2,1)S(1)} %add_convert_fusion), channel_id=1, replica_groups={{0,4,16,20,32,36,48,52},{2,6,18,22,34,38,50,54},{8,12,24,28,40,44,56,60..., dimensions={0} | all-to-all | bytes 524288 | tf_op jit(solution)/shard_map/all_to_all | solution.py:85
  122.1 0.8 shard_map.147
  (53 shorter events, 7.0 us)
Async XLA Ops:
  0.6 1.5 %collective-permute-start = (bf16[64,256]{1,0:T(8,128)(2,1)}, bf16[64,256]{1,0:T(8,128)(2,1)S(1)}, u32[]{:S(2)}, u32[]{:S(2)}) collective-permute-start(bf16[64,256]{1,0:T(8,128)(2,1)} %bitcast.19), channel_id=1, source_target_pairs={{0,1},{1,0},{2,3},{3,2},{4,5},{5,4},{6,7},{7,6},{8,9},{9,8},{10,11... | collective-permute-start | bytes 98312 | tf_op jit(solution)/shard_map/ppermute | solution.py:40
  3.7 9.3 %collective-permute-start.4 = (bf16[8,8,3200]{2,1,0:T(8,128)(2,1)}, bf16[8,8,3200]{2,1,0:T(8,128)(2,1)}, u32[]{:S(2)}, u32[]{:S(2)}) collective-permute-start(bf16[8,8,3200]{2,1,0:T(8,128)(2,1)} %bitcast.3), channel_id=1, source_target_pairs={{0,10},{1,63},{2,8},{3,61},{4,14},{5,59},{6,12},{7,57},{8,2},{9,23... | collective-permute-start | bytes 1228808 | tf_op jit(solution)/shard_map/ppermute | solution.py:81
  6.5 10.7 %collective-permute-start.5 = (bf16[8,8,3200]{2,1,0:T(8,128)(2,1)}, bf16[8,8,3200]{2,1,0:T(8,128)(2,1)}, u32[]{:S(2)}, u32[]{:S(2)}) collective-permute-start(bf16[8,8,3200]{2,1,0:T(8,128)(2,1)} %bitcast.4), channel_id=1, source_target_pairs={{0,2},{1,7},{2,0},{3,5},{4,6},{5,3},{6,4},{7,1},{8,10},{9,15},{10,... | collective-permute-start | bytes 1228808 | tf_op jit(solution)/shard_map/ppermute | solution.py:81
  7.0 10.2 %collective-permute-start.6 = (bf16[8,8,3200]{2,1,0:T(8,128)(2,1)S(1)}, bf16[8,8,3200]{2,1,0:T(8,128)(2,1)}, u32[]{:S(2)}, u32[]{:S(2)}) collective-permute-start(bf16[8,8,3200]{2,1,0:T(8,128)(2,1)S(1)} %bitcast.17), channel_id=1, source_target_pairs={{0,8},{1,57},{2,10},{3,59},{4,12},{5,61},{6,14},{7,63},{8,0},{9,17... | collective-permute-start | bytes 1228808 | tf_op jit(solution)/shard_map/ppermute | solution.py:81
  7.9 1.6 %copy-start.2 = (f32[8,8,64,128]{3,2,1,0:T(8,128)S(1)}, f32[8,8,64,128]{3,2,1,0:T(8,128)}, u32[]{:S(2)}) copy-start(f32[8,8,64,128]{3,2,1,0:T(8,128)} %param.23) | copy-start | bytes 6291460
  9.7 20.3 %copy-start.3 = (bf16[1024,128]{1,0:T(8,128)(2,1)S(1)}, bf16[1024,128]{1,0:T(8,128)(2,1)}, u32[]{:S(2)}) copy-start(bf16[1024,128]{1,0:T(8,128)(2,1)} %w_mix.3) | copy-start | bytes 786436
  19.5 23.6 %all-to-all-start = ((bf16[8,8,3200]{2,1,0:T(8,128)(2,1)}), bf16[8,8,3200]{2,1,0:T(8,128)(2,1)S(1)}, u32[]{:S(2)}, u32[]{:S(2)}) async-start(bf16[8,8,3200]{2,1,0:T(8,128)(2,1)} %fusion.2), calls=%async_computation | async-start | bytes 819200 | tf_op jit(solution)/shard_map/all_to_all | solution.py:85
  31.0 28.1 %collective-permute-start.1 = (bf16[1088,128]{1,0:T(8,128)(2,1)}, bf16[1088,128]{1,0:T(8,128)(2,1)S(1)}, u32[]{:S(2)}, u32[]{:S(2)}) collective-permute-start(bf16[1088,128]{1,0:T(8,128)(2,1)} %get-tuple-element.44), channel_id=1, source_target_pairs={{0,2},{1,3},{2,0},{3,1},{4,6},{5,7},{6,4},{7,5},{8,10},{9,11},{10,... | collective-permute-start | bytes 835592 | tf_op jit(solution)/shard_map/ppermute | solution.py:81
  31.6 27.6 %collective-permute-start.2 = (bf16[1088,128]{1,0:T(8,128)(2,1)}, bf16[1088,128]{1,0:T(8,128)(2,1)S(1)}, u32[]{:S(2)}, u32[]{:S(2)}) collective-permute-start(bf16[1088,128]{1,0:T(8,128)(2,1)} %get-tuple-element.45), channel_id=1, source_target_pairs={{0,8},{1,9},{2,10},{3,11},{4,12},{5,13},{6,14},{7,15},{8,0},{9,1},... | collective-permute-start | bytes 835592 | tf_op jit(solution)/shard_map/ppermute | solution.py:81
  32.6 26.5 %collective-permute-start.3 = (bf16[1088,128]{1,0:T(8,128)(2,1)}, bf16[1088,128]{1,0:T(8,128)(2,1)S(1)}, u32[]{:S(2)}, u32[]{:S(2)}) collective-permute-start(bf16[1088,128]{1,0:T(8,128)(2,1)} %get-tuple-element.46), channel_id=1, source_target_pairs={{0,10},{1,11},{2,8},{3,9},{4,14},{5,15},{6,12},{7,13},{8,2},{9,3},... | collective-permute-start | bytes 835592 | tf_op jit(solution)/shard_map/ppermute | solution.py:81
  43.1 16.1 %copy-start.4 = (bf16[1024,128]{1,0:T(8,128)(2,1)S(1)}, bf16[1024,128]{1,0:T(8,128)(2,1)}, u32[]{:S(2)}) copy-start(bf16[1024,128]{1,0:T(8,128)(2,1)} %w_mix.3) | copy-start | bytes 786436
  43.9 44.3 %copy-start.1 = (bf16[4096,256]{1,0:T(8,128)(2,1)S(1)}, bf16[4096,256]{1,0:T(8,128)(2,1)}, u32[]{:S(2)}) copy-start(bf16[4096,256]{1,0:T(8,128)(2,1)} %refs_5_.5) | copy-start | bytes 6291460
  43.9 44.3 %copy-start.5 = (f32[4096]{0:T(1024)S(1)}, f32[4096]{0:T(1024)}, u32[]{:S(2)}) copy-start(f32[4096]{0:T(1024)} %param.14) | copy-start | bytes 49156
  59.5 1.3 %collective-permute-start.7 = (bf16[4,32,128]{2,1,0:T(8,128)(2,1)S(1)}, bf16[4,32,128]{2,1,0:T(8,128)(2,1)S(1)}, u32[]{:S(2)}, u32[]{:S(2)}) collective-permute-start(bf16[4,32,128]{2,1,0:T(8,128)(2,1)S(1)} %get-tuple-element.57), channel_id=1, source_target_pairs={{0,1},{1,0},{2,3},{3,2},{4,5},{5,4},{6,7},{7,6},{8,9},{9,8},{10,11... | collective-permute-start | bytes 98312 | tf_op jit(solution)/shard_map/ppermute | solution.py:40
  77.6 6.4 %collective-permute-start.11 = (bf16[8,4,32,128]{3,2,1,0:T(8,128)(2,1)S(1)}, bf16[8,4,32,128]{3,2,1,0:T(8,128)(2,1)S(1)}, u32[]{:S(2)}, u32[]{:S(2)}) collective-permute-start(bf16[8,4,32,128]{3,2,1,0:T(8,128)(2,1)S(1)} %all_to_all.21.refs_0_), channel_id=1, source_target_pairs={{0,2},{1,7},{2,0},{3,5},{4,6},{5,3},{6,4},{7,1},{8,10},{9,15},{10,... | collective-permute-start | bytes 786440 | tf_op jit(solution)/shard_map/ppermute | solution.py:81
  78.5 6.4 %collective-permute-start.12 = (bf16[8,4,32,128]{3,2,1,0:T(8,128)(2,1)S(1)}, bf16[8,4,32,128]{3,2,1,0:T(8,128)(2,1)S(1)}, u32[]{:S(2)}, u32[]{:S(2)}) collective-permute-start(bf16[8,4,32,128]{3,2,1,0:T(8,128)(2,1)S(1)} %all_to_all.21.refs_0_), channel_id=1, source_target_pairs={{0,8},{1,57},{2,10},{3,59},{4,12},{5,61},{6,14},{7,63},{8,0},{9,17... | collective-permute-start | bytes 786440 | tf_op jit(solution)/shard_map/ppermute | solution.py:81
  78.5 9.7 %collective-permute-start.8 = (bf16[8,4,32,128]{3,2,1,0:T(8,128)(2,1)S(1)}, bf16[8,4,32,128]{3,2,1,0:T(8,128)(2,1)S(1)}, u32[]{:S(2)}, u32[]{:S(2)}) collective-permute-start(bf16[8,4,32,128]{3,2,1,0:T(8,128)(2,1)S(1)} %all_to_all.21.refs_0_), channel_id=1, source_target_pairs={{0,10},{1,63},{2,8},{3,61},{4,14},{5,59},{6,12},{7,57},{8,2},{9,23... | collective-permute-start | bytes 786440 | tf_op jit(solution)/shard_map/ppermute | solution.py:81
  84.0 4.3 %collective-permute-start.13 = (bf16[8,4,32,128]{3,2,1,0:T(8,128)(2,1)S(1)}, bf16[8,4,32,128]{3,2,1,0:T(8,128)(2,1)S(1)}, u32[]{:S(2)}, u32[]{:S(2)}) collective-permute-start(bf16[8,4,32,128]{3,2,1,0:T(8,128)(2,1)S(1)} %collective-permute-done.11.refs_0_.refs_1_), channel_id=1, source_target_pairs={{0,1},{1,0},{2,3},{3,2},{4,5},{5,4},{6,7},{7,6},{8,9},{9,8},{10,11... | collective-permute-start | bytes 786440 | tf_op jit(solution)/shard_map/ppermute | solution.py:40
  84.9 3.3 %collective-permute-start.14 = (bf16[8,4,32,128]{3,2,1,0:T(8,128)(2,1)S(1)}, bf16[8,4,32,128]{3,2,1,0:T(8,128)(2,1)S(1)}, u32[]{:S(2)}, u32[]{:S(2)}) collective-permute-start(bf16[8,4,32,128]{3,2,1,0:T(8,128)(2,1)S(1)} %collective-permute-done.12.refs_1_.refs_2_), channel_id=1, source_target_pairs={{0,1},{1,0},{2,3},{3,2},{4,5},{5,4},{6,7},{7,6},{8,9},{9,8},{10,11... | collective-permute-start | bytes 786440 | tf_op jit(solution)/shard_map/ppermute | solution.py:40
  84.9 3.9 %collective-permute-start.9 = (bf16[8,4,32,128]{3,2,1,0:T(8,128)(2,1)S(1)}, bf16[8,4,32,128]{3,2,1,0:T(8,128)(2,1)S(1)}, u32[]{:S(2)}, u32[]{:S(2)}) collective-permute-start(bf16[8,4,32,128]{3,2,1,0:T(8,128)(2,1)S(1)} %all_to_all.21.refs_0_), channel_id=1, source_target_pairs={{0,1},{1,0},{2,3},{3,2},{4,5},{5,4},{6,7},{7,6},{8,9},{9,8},{10,11... | collective-permute-start | bytes 786440 | tf_op jit(solution)/shard_map/ppermute | solution.py:40
  88.2 1.5 %collective-permute-start.10 = (bf16[8,4,32,128]{3,2,1,0:T(8,128)(2,1)S(1)}, bf16[8,4,32,128]{3,2,1,0:T(8,128)(2,1)S(1)}, u32[]{:S(2)}, u32[]{:S(2)}) collective-permute-start(bf16[8,4,32,128]{3,2,1,0:T(8,128)(2,1)S(1)} %collective-permute-done.8.refs_1_.refs_3_), channel_id=1, source_target_pairs={{0,1},{1,0},{2,3},{3,2},{4,5},{5,4},{6,7},{7,6},{8,9},{9,8},{10,11... | collective-permute-start | bytes 786440 | tf_op jit(solution)/shard_map/ppermute | solution.py:40
  88.7 1.6 %copy-start = (bf16[256,4096]{1,0:T(8,128)(2,1)S(1)}, bf16[256,4096]{1,0:T(8,128)(2,1)}, u32[]{:S(2)}) copy-start(bf16[256,4096]{1,0:T(8,128)(2,1)} %refs_1_.5) | copy-start | bytes 6291460
  90.9 3.0 %collective-permute-start.16 = (bf16[8,128,128]{2,1,0:T(8,128)(2,1)S(1)}, bf16[8,128,128]{2,1,0:T(8,128)(2,1)S(1)}, u32[]{:S(2)}, u32[]{:S(2)}) collective-permute-start(bf16[8,128,128]{2,1,0:T(8,128)(2,1)S(1)} %get-tuple-element.62), channel_id=1, source_target_pairs={{0,1},{1,0},{2,3},{3,2},{4,5},{5,4},{6,7},{7,6},{8,9},{9,8},{10,11... | collective-permute-start | bytes 786440 | tf_op jit(solution)/shard_map/ppermute | solution.py:40
  92.0 2.4 %collective-permute-start.18 = (bf16[8,128,128]{2,1,0:T(8,128)(2,1)S(1)}, bf16[8,128,128]{2,1,0:T(8,128)(2,1)S(1)}, u32[]{:S(2)}, u32[]{:S(2)}) collective-permute-start(bf16[8,128,128]{2,1,0:T(8,128)(2,1)S(1)} %get-tuple-element.64), channel_id=1, source_target_pairs={{0,1},{1,0},{2,3},{3,2},{4,5},{5,4},{6,7},{7,6},{8,9},{9,8},{10,11... | collective-permute-start | bytes 786440 | tf_op jit(solution)/shard_map/ppermute | solution.py:40
  92.6 3.1 %collective-permute-start.20 = (bf16[8,128,128]{2,1,0:T(8,128)(2,1)S(1)}, bf16[8,128,128]{2,1,0:T(8,128)(2,1)S(1)}, u32[]{:S(2)}, u32[]{:S(2)}) collective-permute-start(bf16[8,128,128]{2,1,0:T(8,128)(2,1)S(1)} %get-tuple-element.66), channel_id=1, source_target_pairs={{0,1},{1,0},{2,3},{3,2},{4,5},{5,4},{6,7},{7,6},{8,9},{9,8},{10,11... | collective-permute-start | bytes 786440 | tf_op jit(solution)/shard_map/ppermute | solution.py:40
  93.7 6.1 %collective-permute-start.15 = (bf16[8,128,128]{2,1,0:T(8,128)(2,1)S(1)}, bf16[8,128,128]{2,1,0:T(8,128)(2,1)S(1)}, u32[]{:S(2)}, u32[]{:S(2)}) collective-permute-start(bf16[8,128,128]{2,1,0:T(8,128)(2,1)S(1)} %get-tuple-element.60), channel_id=1, source_target_pairs={{0,1},{1,0},{2,3},{3,2},{4,5},{5,4},{6,7},{7,6},{8,9},{9,8},{10,11... | collective-permute-start | bytes 786440 | tf_op jit(solution)/shard_map/ppermute | solution.py:40
  93.9 7.5 %collective-permute-start.17 = (bf16[8,128,128]{2,1,0:T(8,128)(2,1)S(1)}, bf16[8,128,128]{2,1,0:T(8,128)(2,1)S(1)}, u32[]{:S(2)}, u32[]{:S(2)}) collective-permute-start(bf16[8,128,128]{2,1,0:T(8,128)(2,1)S(1)} %add_convert_fusion.3), channel_id=1, source_target_pairs={{0,10},{1,63},{2,8},{3,61},{4,14},{5,59},{6,12},{7,57},{8,2},{9,23... | collective-permute-start | bytes 786440 | tf_op jit(solution)/shard_map/ppermute | solution.py:81
  94.4 9.3 %collective-permute-start.19 = (bf16[8,128,128]{2,1,0:T(8,128)(2,1)S(1)}, bf16[8,128,128]{2,1,0:T(8,128)(2,1)S(1)}, u32[]{:S(2)}, u32[]{:S(2)}) collective-permute-start(bf16[8,128,128]{2,1,0:T(8,128)(2,1)S(1)} %add_convert_fusion.2), channel_id=1, source_target_pairs={{0,2},{1,7},{2,0},{3,5},{4,6},{5,3},{6,4},{7,1},{8,10},{9,15},{10,... | collective-permute-start | bytes 786440 | tf_op jit(solution)/shard_map/ppermute | solution.py:81
  95.8 7.9 %collective-permute-start.21 = (bf16[8,128,128]{2,1,0:T(8,128)(2,1)S(1)}, bf16[8,128,128]{2,1,0:T(8,128)(2,1)S(1)}, u32[]{:S(2)}, u32[]{:S(2)}) collective-permute-start(bf16[8,128,128]{2,1,0:T(8,128)(2,1)S(1)} %add_convert_fusion.1), channel_id=1, source_target_pairs={{0,8},{1,57},{2,10},{3,59},{4,12},{5,61},{6,14},{7,63},{8,0},{9,17... | collective-permute-start | bytes 786440 | tf_op jit(solution)/shard_map/ppermute | solution.py:81
where the time goes:
time: 123 us
  blocking collectives  50.2 us (41%)
  waiting for transfers between devices  29.1 us (24%)
  starting transfers between devices  26.8 us (22%)
  Pallas kernels  10.9 us (9%)
  other arithmetic  2.55 us (2%)
  local copies, waits for them, and re-layouts  2.51 us (2%)
    all_to_all x3, blocking collectives, in_class(): lax.all_to_all(x, KV_TP, 0, 0, axis_index_groups=class_groups(), tiled=True)  50.2 us
    ppermute x12, waiting for transfers between devices, to_neighbour(): return lax.ppermute(x, KV_TP, pairs)  18.1 us
    ppermute x12, starting transfers between devices, to_neighbour(): return lax.ppermute(x, KV_TP, pairs)  14.2 us
    pallas_call x17, Pallas kernels, kernel_call(): pl.pallas_call(body, out_shape=[jax.ShapeDtypeStruct(*o) for o in outs],...  10.9 us
    all_to_all x1, starting transfers between devices, in_class(): lax.all_to_all(x, KV_TP, 0, 0, axis_index_groups=class_groups(), tiled=True)  10.5 us
    all_to_all x1, waiting for transfers between devices, in_class(): lax.all_to_all(x, KV_TP, 0, 0, axis_index_groups=class_groups(), tiled=True)  8.6 us
  transfers between devices with their start and end apart: 23, of which 12 were waited for; matrix products, arithmetic and copies ran while one was open for 1% of the time, Pallas kernels for 6%

commit v1 on v0

--- a/solution.py
+++ b/solution.py
@@ -491,28 +491,51 @@
         own_resid_body, [((half, cols), F32)], *mine, *other, flops=10**5
     )
     piece = (count, half, cols)
-    chip_sum = {}
-    hidden = None
-    for place in (*PLACES, 0):
-
-        def down_body(*refs, place=place):
-            down_kernel(*refs, place=place, sizes=sizes)
-
-        def first_down_body(*refs, place=place):
-            hidden_ref = refs[-1]
-            hidden_in_order(*refs[:2], hidden_ref, early, late)
-            down_kernel(hidden_ref, *refs[2:-1], place=place, sizes=sizes)
-
-        outs = [(piece, F32), (piece, BF16)]
-        if hidden is None:
-            keep, send, hidden = kernel_call(
-                first_down_body, [*outs, ((rows, w_up.shape[1]), BF16)], *hiddens, w_down
+
+    def first_down_body(*refs):
+        hidden_ref = refs[-1]
+        hidden_in_order(*refs[:2], hidden_ref, early, late)
+        down_kernel(hidden_ref, *refs[2:-1], place=3, sizes=sizes)
+
+    def pair_down_body(hidden_ref, weights, keep_ref, send_ref):
+        for i, place in enumerate((1, 2)):
+            down_kernel(
+                hidden_ref, weights, keep_ref.at[i], send_ref.at[i], place=place, sizes=sizes
             )
-        else:
-            keep, send = kernel_call(
-                down_body, outs, hidden, w_down, flops=10**7, bytes_accessed=2**21
-            )
-        chip_sum[place] = (keep + swap_tp(send).astype(F32)).astype(BF16)
+
+    def own_down_body(*refs):
+        down_kernel(*refs, place=0, sizes=sizes)
+
+    def chip_total(keep, send):
+        return (keep + swap_tp(send).astype(F32)).astype(BF16)
+
+    keep, send, hidden = kernel_call(
+        first_down_body,
+        [(piece, F32), (piece, BF16), ((rows, w_up.shape[1]), BF16)],
+        *hiddens,
+        w_down,
+    )
+    chip_sum = {3: chip_total(keep, send)}
+    keep, send = kernel_call(
+        pair_down_body,
+        [((2, *piece), F32), ((2, *piece), BF16)],
+        hidden,
+        w_down,
+        flops=2 * 10**7,
+        bytes_accessed=2**22,
+    )
+    received = swap_tp(send)
+    for i, place in enumerate((1, 2)):
+        chip_sum[place] = (keep[i] + received[i].astype(F32)).astype(BF16)
+    keep, send = kernel_call(
+        own_down_body,
+        [(piece, F32), (piece, BF16)],
+        hidden,
+        w_down,
+        flops=10**7,
+        bytes_accessed=2**21,
+    )
+    chip_sum[0] = chip_total(keep, send)
     total, own_resid, new_state = lax.optimization_barrier(
         (sum_in_square(chip_sum), own_resid, new_state)
     )

time: 123 us -> 124 us (level)
  the two profiles are of different devices: /device:TPU:80 before, /device:TPU:18 now
where the time goes in v1:
time: 124 us; the launch traced here: 121 us
  blocking collectives  44.9 us (36%)
  waiting for transfers between devices  33.6 us (27%)
  starting transfers between devices  26.5 us (21%)
  Pallas kernels  10.7 us (9%)
  other arithmetic  2.55 us (2%)
  local copies, waits for them, and re-layouts  2.51 us (2%)
    all_to_all x3, blocking collectives, in_class(): lax.all_to_all(x, KV_TP, 0, 0, axis_index_groups=class_groups(), tiled=True)  44.9 us
    ppermute x12, waiting for transfers between devices, to_neighbour(): return lax.ppermute(x, KV_TP, pairs)  18.6 us
    ppermute x12, starting transfers between devices, to_neighbour(): return lax.ppermute(x, KV_TP, pairs)  14.5 us
    all_to_all x1, waiting for transfers between devices, in_class(): lax.all_to_all(x, KV_TP, 0, 0, axis_index_groups=class_groups(), tiled=True)  11.8 us
    pallas_call x16, Pallas kernels, kernel_call(): pl.pallas_call(body, out_shape=[jax.ShapeDtypeStruct(*o) for o in outs],...  10.7 us
    all_to_all x1, starting transfers between devices, in_class(): lax.all_to_all(x, KV_TP, 0, 0, axis_index_groups=class_groups(), tiled=True)  10 us
    ppermute x9, waiting for transfers between devices, swap_tp(): return lax.ppermute(x, 'tp', [(0, 1), (1, 0)])  3.14 us
  transfers between devices with their start and end apart: 22, of which 12 were waited for; matrix products, arithmetic and copies ran while one was open for 1% of the time, Pallas kernels for 5%

profile of v1, /device:TPU:18, one launch (start us, length us, event | category | flops | bytes accessed | tf_op | source)
XLA Modules:
  0.0 121.5 jit_solution(7703224864518003746)
XLA Ops:
  0.7 1.2 %shard_map.131 = (bf16[64,256]{1,0:T(8,128)(2,1)S(1)}, f32[32,128]{1,0:T(8,128)S(1)}, bf16[128,512]{1,0:T(8,128)(2,1)S(1)}, bf16[128,512]{1,0:T(8,128)(2,1)S(1)}...) custom-call(bf16[64,256]{1,0:T(8,128)(2,1)} %bitcast.24, f32[32,128]{1,0:T(8,128)} %bitcast.26, ...), custom_call_target="tpu_custom_call" | custom-call | flops 10000000 | bytes 2097152 | tf_op jit(solution)/shard_map/pallas_call | solution.py:26
  2.1 1.5 %shard_map.132 = (bf16[64,3200]{1,0:T(8,128)(2,1)S(1)}, bf16[64,3200]{1,0:T(8,128)(2,1)}, bf16[64,3200]{1,0:T(8,128)(2,1)S(1)}, bf16[64,3200]{1,0:T(8,128)(2,1)}, bf16[4,64,128]{2,1,0:T(8,128)(2,1)S(1)}) custom-call(bf16[64,256]{1,0:T(8,128)(2,1)S(1)} %collective-permute-done.refs_0_, bf16[64,256]{1,0:T(8,128)(2,1)S(1)} %get-tuple-element.35.refs_1_, ...), custom_call_target="tpu_custom_call" | custom-call | tf_op jit(solution)/shard_map/pallas_call | solution.py:26
  3.7 1.9 %collective-permute-start.4 = (bf16[8,8,3200]{2,1,0:T(8,128)(2,1)}, bf16[8,8,3200]{2,1,0:T(8,128)(2,1)}, u32[]{:S(2)}, u32[]{:S(2)}) collective-permute-start(bf16[8,8,3200]{2,1,0:T(8,128)(2,1)} %bitcast.3), channel_id=1, source_target_pairs={{0,10},{1,63},{2,8},{3,61},{4,14},{5,59},{6,12},{7,57},{8,2},{9,23... | collective-permute-start | bytes 1228808 | tf_op jit(solution)/shard_map/ppermute | solution.py:81
  5.5 1.5 %collective-permute-start.5 = (bf16[8,8,3200]{2,1,0:T(8,128)(2,1)}, bf16[8,8,3200]{2,1,0:T(8,128)(2,1)}, u32[]{:S(2)}, u32[]{:S(2)}) collective-permute-start(bf16[8,8,3200]{2,1,0:T(8,128)(2,1)} %bitcast.4), channel_id=1, source_target_pairs={{0,2},{1,7},{2,0},{3,5},{4,6},{5,3},{6,4},{7,1},{8,10},{9,15},{10,... | collective-permute-start | bytes 1228808 | tf_op jit(solution)/shard_map/ppermute | solution.py:81
  8.0 1.6 %copy-done.2 = f32[8,8,64,128]{3,2,1,0:T(8,128)S(1)} copy-done((f32[8,8,64,128]{3,2,1,0:T(8,128)S(1)}, f32[8,8,64,128]{3,2,1,0:T(8,128)}, u32[]{:S(2)}) %copy-start.2) | copy-done | bytes 2097176
  9.7 3.2 %collective-permute-done.4 = bf16[8,8,3200]{2,1,0:T(8,128)(2,1)} collective-permute-done((bf16[8,8,3200]{2,1,0:T(8,128)(2,1)}, bf16[8,8,3200]{2,1,0:T(8,128)(2,1)}, u32[]{:S(2)}, u32[]{:S(2)}) %collective-permute-start.4) | collective-permute-done | bytes 409632 | tf_op jit(solution)/shard_map/ppermute | solution.py:81
  12.9 4.3 %collective-permute-done.5 = bf16[8,8,3200]{2,1,0:T(8,128)(2,1)} collective-permute-done((bf16[8,8,3200]{2,1,0:T(8,128)(2,1)}, bf16[8,8,3200]{2,1,0:T(8,128)(2,1)}, u32[]{:S(2)}, u32[]{:S(2)}) %collective-permute-start.5) | collective-permute-done | bytes 409632 | tf_op jit(solution)/shard_map/ppermute | solution.py:81
  17.2 2.2 %fusion.2 = bf16[8,8,3200]{2,1,0:T(8,128)(2,1)} fusion(bf16[8,8,3200]{2,1,0:T(8,128)(2,1)} %collective-permute-done.6, bf16[8,8,3200]{2,1,0:T(8,128)(2,1)} %collective-permute-done.5, bf16[8,8,3200]{2,1,0:T(8,128)(2,1)} %collective-permute-done.4, bf16[64,3200]{1,0:T(8,128)(2,1)S(1)} %get-tuple-element.45), kind=kLoop, calls=%fused_computation.3 | loop fusion | flops 1638400 | bytes 2048000 | tf_op jit(solution)/shard_map/convert_element_type | solution.py:98
  19.4 10.0 %all-to-all-start = ((bf16[8,8,3200]{2,1,0:T(8,128)(2,1)}), bf16[8,8,3200]{2,1,0:T(8,128)(2,1)S(1)}, u32[]{:S(2)}, u32[]{:S(2)}) async-start(bf16[8,8,3200]{2,1,0:T(8,128)(2,1)} %fusion.2), calls=%async_computation | async-start | bytes 819200 | tf_op jit(solution)/shard_map/all_to_all | solution.py:85
  29.5 1.0 shard_map.134
  30.5 1.4 %collective-permute-start.1 = (bf16[1088,128]{1,0:T(8,128)(2,1)}, bf16[1088,128]{1,0:T(8,128)(2,1)S(1)}, u32[]{:S(2)}, u32[]{:S(2)}) collective-permute-start(bf16[1088,128]{1,0:T(8,128)(2,1)} %get-tuple-element.42), channel_id=1, source_target_pairs={{0,2},{1,3},{2,0},{3,1},{4,6},{5,7},{6,4},{7,5},{8,10},{9,11},{10,... | collective-permute-start | bytes 835592 | tf_op jit(solution)/shard_map/ppermute | solution.py:81
  31.9 1.0 collective-permute-start.2
  32.9 1.0 collective-permute-start.3
  34.0 11.8 %all-to-all-done.refs_0_ = bf16[8,8,3200]{2,1,0:T(8,128)(2,1)S(1)} async-done(((bf16[8,8,3200]{2,1,0:T(8,128)(2,1)}), bf16[8,8,3200]{2,1,0:T(8,128)(2,1)S(1)}, u32[]{:S(2)}, u32[]{:S(2)}) %all-to-all-start) | async-done | bytes 409632 | tf_op jit(solution)/shard_map/all_to_all | solution.py:85
  45.8 0.8 shard_map.136
  46.7 14.2 %all_to_all.20 = bf16[8,8,1024]{2,1,0:T(8,128)(2,1)S(1)} all-to-all(bf16[8,8,1024]{2,1,0:T(8,128)(2,1)S(1)} %get-tuple-element.52), channel_id=1, replica_groups={{0,4,16,20,32,36,48,52},{2,6,18,22,34,38,50,54},{8,12,24,28,40,44,56,60..., dimensions={0} | all-to-all | bytes 262144 | tf_op jit(solution)/shard_map/all_to_all | solution.py:85
  61.3 1.2 collective-permute-done.7.rest_4_
  62.5 13.8 %all_to_all.21.refs_0_ = bf16[8,4,32,128]{3,2,1,0:T(8,128)(2,1)S(1)} all-to-all(bf16[8,4,32,128]{3,2,1,0:T(8,128)(2,1)S(1)} %shard_map.138), channel_id=1, replica_groups={{0,4,16,20,32,36,48,52},{2,6,18,22,34,38,50,54},{8,12,24,28,40,44,56,60..., dimensions={0} | all-to-all | bytes 524288 | tf_op jit(solution)/shard_map/all_to_all | solution.py:85
  76.3 1.5 %collective-permute-start.11 = (bf16[8,4,32,128]{3,2,1,0:T(8,128)(2,1)S(1)}, bf16[8,4,32,128]{3,2,1,0:T(8,128)(2,1)S(1)}, u32[]{:S(2)}, u32[]{:S(2)}) collective-permute-start(bf16[8,4,32,128]{3,2,1,0:T(8,128)(2,1)S(1)} %all_to_all.21.refs_0_), channel_id=1, source_target_pairs={{0,2},{1,7},{2,0},{3,5},{4,6},{5,3},{6,4},{7,1},{8,10},{9,15},{10,... | collective-permute-start | bytes 786440 | tf_op jit(solution)/shard_map/ppermute | solution.py:81
  77.8 2.4 %collective-permute-start.12 = (bf16[8,4,32,128]{3,2,1,0:T(8,128)(2,1)S(1)}, bf16[8,4,32,128]{3,2,1,0:T(8,128)(2,1)S(1)}, u32[]{:S(2)}, u32[]{:S(2)}) collective-permute-start(bf16[8,4,32,128]{3,2,1,0:T(8,128)(2,1)S(1)} %all_to_all.21.refs_0_), channel_id=1, source_target_pairs={{0,8},{1,57},{2,10},{3,59},{4,12},{5,61},{6,14},{7,63},{8,0},{9,17... | collective-permute-start | bytes 786440 | tf_op jit(solution)/shard_map/ppermute | solution.py:81
  80.2 2.5 %collective-permute-done.11.refs_0_.refs_1_ = bf16[8,4,32,128]{3,2,1,0:T(8,128)(2,1)S(1)} collective-permute-done((bf16[8,4,32,128]{3,2,1,0:T(8,128)(2,1)S(1)}, bf16[8,4,32,128]{3,2,1,0:T(8,128)(2,1)S(1)}, u32[]{:S(2)}, u32[]{:S(2)}) %collective-permute-start.11) | collective-permute-done | bytes 262176 | tf_op jit(solution)/shard_map/ppermute | solution.py:81
  82.7 1.9 %collective-permute-done.12.refs_1_.refs_2_ = bf16[8,4,32,128]{3,2,1,0:T(8,128)(2,1)S(1)} collective-permute-done((bf16[8,4,32,128]{3,2,1,0:T(8,128)(2,1)S(1)}, bf16[8,4,32,128]{3,2,1,0:T(8,128)(2,1)S(1)}, u32[]{:S(2)}, u32[]{:S(2)}) %collective-permute-start.12) | collective-permute-done | bytes 262176 | tf_op jit(solution)/shard_map/ppermute | solution.py:81
  85.1 2.4 %collective-permute-done.8.refs_1_.refs_3_ = bf16[8,4,32,128]{3,2,1,0:T(8,128)(2,1)S(1)} collective-permute-done((bf16[8,4,32,128]{3,2,1,0:T(8,128)(2,1)S(1)}, bf16[8,4,32,128]{3,2,1,0:T(8,128)(2,1)S(1)}, u32[]{:S(2)}, u32[]{:S(2)}) %collective-permute-start.8) | collective-permute-done | bytes 262176 | tf_op jit(solution)/shard_map/ppermute | solution.py:81
  88.0 1.0 collective-permute-done.10.refs_3_.refs_7_
  90.1 0.8 shard_map.143
  92.6 0.8 collective-permute-done.16
  93.5 2.9 %collective-permute-start.17 = (bf16[8,128,128]{2,1,0:T(8,128)(2,1)S(1)}, bf16[8,128,128]{2,1,0:T(8,128)(2,1)S(1)}, u32[]{:S(2)}, u32[]{:S(2)}) collective-permute-start(bf16[8,128,128]{2,1,0:T(8,128)(2,1)S(1)} %add_convert_fusion.3), channel_id=1, source_target_pairs={{0,10},{1,63},{2,8},{3,61},{4,14},{5,59},{6,12},{7,57},{8,2},{9,23... | collective-permute-start | bytes 786440 | tf_op jit(solution)/shard_map/ppermute | solution.py:81
  97.3 1.9 %shard_map.145 = f32[64,64,128]{2,1,0:T(8,128)} custom-call(f32[64,64,128]{2,1,0:T(8,128)S(1)} %shard_map.135.refs_1_.decayed, f32[512,8]{1,0:T(8,128)S(1)} %get-tuple-element.63.key_t, f32[8,1024]{1,0:T(8,128)S(1)} %get-tuple-element.64.value), custom_call_target="tpu_custom_call" | custom-call | flops 30000000 | bytes 8388608 | tf_op jit(solution)/shard_map/pallas_call | solution.py:26
  99.3 1.6 %collective-permute-done.17 = bf16[8,128,128]{2,1,0:T(8,128)(2,1)S(1)} collective-permute-done((bf16[8,128,128]{2,1,0:T(8,128)(2,1)S(1)}, bf16[8,128,128]{2,1,0:T(8,128)(2,1)S(1)}, u32[]{:S(2)}, u32[]{:S(2)}) %collective-permute-start.17) | collective-permute-done | bytes 262176 | tf_op jit(solution)/shard_map/ppermute | solution.py:81
  100.9 2.7 %collective-permute-done.19 = bf16[8,128,128]{2,1,0:T(8,128)(2,1)S(1)} collective-permute-done((bf16[8,128,128]{2,1,0:T(8,128)(2,1)S(1)}, bf16[8,128,128]{2,1,0:T(8,128)(2,1)S(1)}, u32[]{:S(2)}, u32[]{:S(2)}) %collective-permute-start.19) | collective-permute-done | bytes 262176 | tf_op jit(solution)/shard_map/ppermute | solution.py:81
  103.8 16.9 %all_to_all.22.refs_0_ = bf16[8,128,128]{2,1,0:T(8,128)(2,1)S(1)} all-to-all(bf16[8,128,128]{2,1,0:T(8,128)(2,1)S(1)} %add_convert_fusion), channel_id=1, replica_groups={{0,4,16,20,32,36,48,52},{2,6,18,22,34,38,50,54},{8,12,24,28,40,44,56,60..., dimensions={0} | all-to-all | bytes 524288 | tf_op jit(solution)/shard_map/all_to_all | solution.py:85
  120.7 0.8 shard_map.146
  (49 shorter events, 6.8 us)
Async XLA Ops:
  0.6 1.5 %collective-permute-start = (bf16[64,256]{1,0:T(8,128)(2,1)}, bf16[64,256]{1,0:T(8,128)(2,1)S(1)}, u32[]{:S(2)}, u32[]{:S(2)}) collective-permute-start(bf16[64,256]{1,0:T(8,128)(2,1)} %bitcast.23), channel_id=1, source_target_pairs={{0,1},{1,0},{2,3},{3,2},{4,5},{5,4},{6,7},{7,6},{8,9},{9,8},{10,11... | collective-permute-start | bytes 98312 | tf_op jit(solution)/shard_map/ppermute | solution.py:40
  3.7 9.3 %collective-permute-start.4 = (bf16[8,8,3200]{2,1,0:T(8,128)(2,1)}, bf16[8,8,3200]{2,1,0:T(8,128)(2,1)}, u32[]{:S(2)}, u32[]{:S(2)}) collective-permute-start(bf16[8,8,3200]{2,1,0:T(8,128)(2,1)} %bitcast.3), channel_id=1, source_target_pairs={{0,10},{1,63},{2,8},{3,61},{4,14},{5,59},{6,12},{7,57},{8,2},{9,23... | collective-permute-start | bytes 1228808 | tf_op jit(solution)/shard_map/ppermute | solution.py:81
  5.5 11.7 %collective-permute-start.5 = (bf16[8,8,3200]{2,1,0:T(8,128)(2,1)}, bf16[8,8,3200]{2,1,0:T(8,128)(2,1)}, u32[]{:S(2)}, u32[]{:S(2)}) collective-permute-start(bf16[8,8,3200]{2,1,0:T(8,128)(2,1)} %bitcast.4), channel_id=1, source_target_pairs={{0,2},{1,7},{2,0},{3,5},{4,6},{5,3},{6,4},{7,1},{8,10},{9,15},{10,... | collective-permute-start | bytes 1228808 | tf_op jit(solution)/shard_map/ppermute | solution.py:81
  7.0 10.2 %collective-permute-start.6 = (bf16[8,8,3200]{2,1,0:T(8,128)(2,1)S(1)}, bf16[8,8,3200]{2,1,0:T(8,128)(2,1)}, u32[]{:S(2)}, u32[]{:S(2)}) collective-permute-start(bf16[8,8,3200]{2,1,0:T(8,128)(2,1)S(1)} %bitcast.21), channel_id=1, source_target_pairs={{0,8},{1,57},{2,10},{3,59},{4,12},{5,61},{6,14},{7,63},{8,0},{9,17... | collective-permute-start | bytes 1228808 | tf_op jit(solution)/shard_map/ppermute | solution.py:81
  7.9 1.6 %copy-start.2 = (f32[8,8,64,128]{3,2,1,0:T(8,128)S(1)}, f32[8,8,64,128]{3,2,1,0:T(8,128)}, u32[]{:S(2)}) copy-start(f32[8,8,64,128]{3,2,1,0:T(8,128)} %param.23) | copy-start | bytes 6291460
  9.7 19.8 %copy-start.3 = (bf16[1024,128]{1,0:T(8,128)(2,1)S(1)}, bf16[1024,128]{1,0:T(8,128)(2,1)}, u32[]{:S(2)}) copy-start(bf16[1024,128]{1,0:T(8,128)(2,1)} %w_mix.3) | copy-start | bytes 786436
  19.4 26.4 %all-to-all-start = ((bf16[8,8,3200]{2,1,0:T(8,128)(2,1)}), bf16[8,8,3200]{2,1,0:T(8,128)(2,1)S(1)}, u32[]{:S(2)}, u32[]{:S(2)}) async-start(bf16[8,8,3200]{2,1,0:T(8,128)(2,1)} %fusion.2), calls=%async_computation | async-start | bytes 819200 | tf_op jit(solution)/shard_map/all_to_all | solution.py:85
  30.5 30.4 %collective-permute-start.1 = (bf16[1088,128]{1,0:T(8,128)(2,1)}, bf16[1088,128]{1,0:T(8,128)(2,1)S(1)}, u32[]{:S(2)}, u32[]{:S(2)}) collective-permute-start(bf16[1088,128]{1,0:T(8,128)(2,1)} %get-tuple-element.42), channel_id=1, source_target_pairs={{0,2},{1,3},{2,0},{3,1},{4,6},{5,7},{6,4},{7,5},{8,10},{9,11},{10,... | collective-permute-start | bytes 835592 | tf_op jit(solution)/shard_map/ppermute | solution.py:81
  31.9 28.9 %collective-permute-start.2 = (bf16[1088,128]{1,0:T(8,128)(2,1)}, bf16[1088,128]{1,0:T(8,128)(2,1)S(1)}, u32[]{:S(2)}, u32[]{:S(2)}) collective-permute-start(bf16[1088,128]{1,0:T(8,128)(2,1)} %get-tuple-element.43), channel_id=1, source_target_pairs={{0,8},{1,9},{2,10},{3,11},{4,12},{5,13},{6,14},{7,15},{8,0},{9,1},... | collective-permute-start | bytes 835592 | tf_op jit(solution)/shard_map/ppermute | solution.py:81
  32.9 27.9 %collective-permute-start.3 = (bf16[1088,128]{1,0:T(8,128)(2,1)}, bf16[1088,128]{1,0:T(8,128)(2,1)S(1)}, u32[]{:S(2)}, u32[]{:S(2)}) collective-permute-start(bf16[1088,128]{1,0:T(8,128)(2,1)} %get-tuple-element.44), channel_id=1, source_target_pairs={{0,10},{1,11},{2,8},{3,9},{4,14},{5,15},{6,12},{7,13},{8,2},{9,3},... | collective-permute-start | bytes 835592 | tf_op jit(solution)/shard_map/ppermute | solution.py:81
  45.8 15.0 %copy-start.4 = (bf16[1024,128]{1,0:T(8,128)(2,1)S(1)}, bf16[1024,128]{1,0:T(8,128)(2,1)}, u32[]{:S(2)}) copy-start(bf16[1024,128]{1,0:T(8,128)(2,1)} %w_mix.3) | copy-start | bytes 786436
  46.6 40.9 %copy-start.1 = (bf16[4096,256]{1,0:T(8,128)(2,1)S(1)}, bf16[4096,256]{1,0:T(8,128)(2,1)}, u32[]{:S(2)}) copy-start(bf16[4096,256]{1,0:T(8,128)(2,1)} %refs_5_.5) | copy-start | bytes 6291460
  46.6 40.8 %copy-start.5 = (f32[4096]{0:T(1024)S(1)}, f32[4096]{0:T(1024)}, u32[]{:S(2)}) copy-start(f32[4096]{0:T(1024)} %param.14) | copy-start | bytes 49156
  61.2 1.3 %collective-permute-start.7 = (bf16[4,32,128]{2,1,0:T(8,128)(2,1)S(1)}, bf16[4,32,128]{2,1,0:T(8,128)(2,1)S(1)}, u32[]{:S(2)}, u32[]{:S(2)}) collective-permute-start(bf16[4,32,128]{2,1,0:T(8,128)(2,1)S(1)} %get-tuple-element.55), channel_id=1, source_target_pairs={{0,1},{1,0},{2,3},{3,2},{4,5},{5,4},{6,7},{7,6},{8,9},{9,8},{10,11... | collective-permute-start | bytes 98312 | tf_op jit(solution)/shard_map/ppermute | solution.py:40
  76.3 6.4 %collective-permute-start.11 = (bf16[8,4,32,128]{3,2,1,0:T(8,128)(2,1)S(1)}, bf16[8,4,32,128]{3,2,1,0:T(8,128)(2,1)S(1)}, u32[]{:S(2)}, u32[]{:S(2)}) collective-permute-start(bf16[8,4,32,128]{3,2,1,0:T(8,128)(2,1)S(1)} %all_to_all.21.refs_0_), channel_id=1, source_target_pairs={{0,2},{1,7},{2,0},{3,5},{4,6},{5,3},{6,4},{7,1},{8,10},{9,15},{10,... | collective-permute-start | bytes 786440 | tf_op jit(solution)/shard_map/ppermute | solution.py:81
  77.8 6.7 %collective-permute-start.12 = (bf16[8,4,32,128]{3,2,1,0:T(8,128)(2,1)S(1)}, bf16[8,4,32,128]{3,2,1,0:T(8,128)(2,1)S(1)}, u32[]{:S(2)}, u32[]{:S(2)}) collective-permute-start(bf16[8,4,32,128]{3,2,1,0:T(8,128)(2,1)S(1)} %all_to_all.21.refs_0_), channel_id=1, source_target_pairs={{0,8},{1,57},{2,10},{3,59},{4,12},{5,61},{6,14},{7,63},{8,0},{9,17... | collective-permute-start | bytes 786440 | tf_op jit(solution)/shard_map/ppermute | solution.py:81
  80.2 7.3 %collective-permute-start.8 = (bf16[8,4,32,128]{3,2,1,0:T(8,128)(2,1)S(1)}, bf16[8,4,32,128]{3,2,1,0:T(8,128)(2,1)S(1)}, u32[]{:S(2)}, u32[]{:S(2)}) collective-permute-start(bf16[8,4,32,128]{3,2,1,0:T(8,128)(2,1)S(1)} %all_to_all.21.refs_0_), channel_id=1, source_target_pairs={{0,10},{1,63},{2,8},{3,61},{4,14},{5,59},{6,12},{7,57},{8,2},{9,23... | collective-permute-start | bytes 786440 | tf_op jit(solution)/shard_map/ppermute | solution.py:81
  82.7 4.8 %collective-permute-start.13 = (bf16[8,4,32,128]{3,2,1,0:T(8,128)(2,1)S(1)}, bf16[8,4,32,128]{3,2,1,0:T(8,128)(2,1)S(1)}, u32[]{:S(2)}, u32[]{:S(2)}) collective-permute-start(bf16[8,4,32,128]{3,2,1,0:T(8,128)(2,1)S(1)} %collective-permute-done.11.refs_0_.refs_1_), channel_id=1, source_target_pairs={{0,1},{1,0},{2,3},{3,2},{4,5},{5,4},{6,7},{7,6},{8,9},{9,8},{10,11... | collective-permute-start | bytes 786440 | tf_op jit(solution)/shard_map/ppermute | solution.py:40
  84.6 2.9 %collective-permute-start.14 = (bf16[8,4,32,128]{3,2,1,0:T(8,128)(2,1)S(1)}, bf16[8,4,32,128]{3,2,1,0:T(8,128)(2,1)S(1)}, u32[]{:S(2)}, u32[]{:S(2)}) collective-permute-start(bf16[8,4,32,128]{3,2,1,0:T(8,128)(2,1)S(1)} %collective-permute-done.12.refs_1_.refs_2_), channel_id=1, source_target_pairs={{0,1},{1,0},{2,3},{3,2},{4,5},{5,4},{6,7},{7,6},{8,9},{9,8},{10,11... | collective-permute-start | bytes 786440 | tf_op jit(solution)/shard_map/ppermute | solution.py:40
  84.6 3.4 %collective-permute-start.9 = (bf16[8,4,32,128]{3,2,1,0:T(8,128)(2,1)S(1)}, bf16[8,4,32,128]{3,2,1,0:T(8,128)(2,1)S(1)}, u32[]{:S(2)}, u32[]{:S(2)}) collective-permute-start(bf16[8,4,32,128]{3,2,1,0:T(8,128)(2,1)S(1)} %all_to_all.21.refs_0_), channel_id=1, source_target_pairs={{0,1},{1,0},{2,3},{3,2},{4,5},{5,4},{6,7},{7,6},{8,9},{9,8},{10,11... | collective-permute-start | bytes 786440 | tf_op jit(solution)/shard_map/ppermute | solution.py:40
  87.5 1.5 %collective-permute-start.10 = (bf16[8,4,32,128]{3,2,1,0:T(8,128)(2,1)S(1)}, bf16[8,4,32,128]{3,2,1,0:T(8,128)(2,1)S(1)}, u32[]{:S(2)}, u32[]{:S(2)}) collective-permute-start(bf16[8,4,32,128]{3,2,1,0:T(8,128)(2,1)S(1)} %collective-permute-done.8.refs_1_.refs_3_), channel_id=1, source_target_pairs={{0,1},{1,0},{2,3},{3,2},{4,5},{5,4},{6,7},{7,6},{8,9},{9,8},{10,11... | collective-permute-start | bytes 786440 | tf_op jit(solution)/shard_map/ppermute | solution.py:40
  88.0 1.6 %copy-start = (bf16[256,4096]{1,0:T(8,128)(2,1)S(1)}, bf16[256,4096]{1,0:T(8,128)(2,1)}, u32[]{:S(2)}) copy-start(bf16[256,4096]{1,0:T(8,128)(2,1)} %weights.1) | copy-start | bytes 6291460
  90.9 5.5 %collective-permute-start.18 = (bf16[2,8,128,128]{3,2,1,0:T(8,128)(2,1)S(1)}, bf16[2,8,128,128]{3,2,1,0:T(8,128)(2,1)S(1)}, u32[]{:S(2)}, u32[]{:S(2)}) collective-permute-start(bf16[2,8,128,128]{3,2,1,0:T(8,128)(2,1)S(1)} %get-tuple-element.62), channel_id=1, source_target_pairs={{0,1},{1,0},{2,3},{3,2},{4,5},{5,4},{6,7},{7,6},{8,9},{9,8},{10,11... | collective-permute-start | bytes 1572872 | tf_op jit(solution)/shard_map/ppermute | solution.py:40
  91.5 1.9 %collective-permute-start.16 = (bf16[8,128,128]{2,1,0:T(8,128)(2,1)S(1)}, bf16[8,128,128]{2,1,0:T(8,128)(2,1)S(1)}, u32[]{:S(2)}, u32[]{:S(2)}) collective-permute-start(bf16[8,128,128]{2,1,0:T(8,128)(2,1)S(1)} %get-tuple-element.60), channel_id=1, source_target_pairs={{0,1},{1,0},{2,3},{3,2},{4,5},{5,4},{6,7},{7,6},{8,9},{9,8},{10,11... | collective-permute-start | bytes 786440 | tf_op jit(solution)/shard_map/ppermute | solution.py:40
  92.1 7.2 %collective-permute-start.15 = (bf16[8,128,128]{2,1,0:T(8,128)(2,1)S(1)}, bf16[8,128,128]{2,1,0:T(8,128)(2,1)S(1)}, u32[]{:S(2)}, u32[]{:S(2)}) collective-permute-start(bf16[8,128,128]{2,1,0:T(8,128)(2,1)S(1)} %get-tuple-element.58), channel_id=1, source_target_pairs={{0,1},{1,0},{2,3},{3,2},{4,5},{5,4},{6,7},{7,6},{8,9},{9,8},{10,11... | collective-permute-start | bytes 786440 | tf_op jit(solution)/shard_map/ppermute | solution.py:40
  93.5 7.4 %collective-permute-start.17 = (bf16[8,128,128]{2,1,0:T(8,128)(2,1)S(1)}, bf16[8,128,128]{2,1,0:T(8,128)(2,1)S(1)}, u32[]{:S(2)}, u32[]{:S(2)}) collective-permute-start(bf16[8,128,128]{2,1,0:T(8,128)(2,1)S(1)} %add_convert_fusion.3), channel_id=1, source_target_pairs={{0,10},{1,63},{2,8},{3,61},{4,14},{5,59},{6,12},{7,57},{8,2},{9,23... | collective-permute-start | bytes 786440 | tf_op jit(solution)/shard_map/ppermute | solution.py:81
  96.5 7.1 %collective-permute-start.19 = (bf16[8,128,128]{2,1,0:T(8,128)(2,1)S(1)}, bf16[8,128,128]{2,1,0:T(8,128)(2,1)S(1)}, u32[]{:S(2)}, u32[]{:S(2)}) collective-permute-start(bf16[8,128,128]{2,1,0:T(8,128)(2,1)S(1)} %get-tuple-element.68), channel_id=1, source_target_pairs={{0,2},{1,7},{2,0},{3,5},{4,6},{5,3},{6,4},{7,1},{8,10},{9,15},{10,... | collective-permute-start | bytes 786440 | tf_op jit(solution)/shard_map/ppermute | solution.py:81
  96.8 6.9 %collective-permute-start.20 = (bf16[8,128,128]{2,1,0:T(8,128)(2,1)S(1)}, bf16[8,128,128]{2,1,0:T(8,128)(2,1)S(1)}, u32[]{:S(2)}, u32[]{:S(2)}) collective-permute-start(bf16[8,128,128]{2,1,0:T(8,128)(2,1)S(1)} %get-tuple-element.69), channel_id=1, source_target_pairs={{0,8},{1,57},{2,10},{3,59},{4,12},{5,61},{6,14},{7,63},{8,0},{9,17... | collective-permute-start | bytes 786440 | tf_op jit(solution)/shard_map/ppermute | solution.py:81
